TPU v7x, 32 devices: a whole 2x2x4 slice. The times are simulated.
32 devices in a mesh: tp: 16 (over z, y, x), dp: 2 (over core).
Axes of the slice: x: 2, y: 2, z: 4, core: 2. Of those that a mesh axis runs over, the one named last changes fastest.
Arguments:
- hidden: bfloat16 [16, 4096], P(None, 'dp'), may hold values from -6 to 6
- norm_gain: float32 [2, 4096], P(None, 'dp'), may hold values from 0.1 to 1.9
- gate_weight: bfloat16 [2, 4096, 8192], P(None, 'dp', 'tp'), may hold values from -0.09375 to 0.09375
- inner_weight: bfloat16 [2, 4096, 8192], P(None, 'dp', 'tp'), may hold values from -0.09375 to 0.09375
- write_weight: bfloat16 [2, 4096, 2048], P(None, 'dp', 'tp'), may hold values from -0.09375 to 0.09375
- read_weight: bfloat16 [2, 4096, 2048], P(None, 'dp', 'tp'), may hold values from -0.09375 to 0.09375
- step_weight: bfloat16 [2, 4096, 128], P(None, 'dp'), may hold values from -0.09375 to 0.09375
- conv_inner: bfloat16 [2, 4, 8192], P(None, None, 'tp'), may hold values from -3 to 3
- conv_write: bfloat16 [2, 4, 2048], P(None, None, 'tp'), may hold values from -3 to 3
- conv_read: bfloat16 [2, 4, 2048], P(None, None, 'tp'), may hold values from -3 to 3
- step_bias: float32 [2, 128], P(None, 'tp'), may hold values from -4 to -1
- decay_log: float32 [2, 128], P(None, 'tp'), may hold values from -3 to 0.5
- skip_gain: float32 [2, 128], P(None, 'tp'), may hold values from 0.1 to 1.9
- group_gain: float32 [2, 8192], P(None, 'tp'), may hold values from 0.1 to 1.9
- out_weight: bfloat16 [2, 8192, 4096], P(None, 'tp', 'dp'), may hold values from -0.4 to 0.4
- state_inner: bfloat16 [2, 16, 3, 8192], P(None, 'dp', None, 'tp'), may hold values from -6 to 6
- state_write: bfloat16 [2, 16, 3, 2048], P(None, 'dp', None, 'tp'), may hold values from -6 to 6
- state_read: bfloat16 [2, 16, 3, 2048], P(None, 'dp', None, 'tp'), may hold values from -6 to 6
- recurrent: float32 [2, 16, 128, 64, 128], P(None, 'dp', 'tp'), may hold values from -1.2 to 1.2, as said below
Outputs:
- out_hidden: bfloat16 [16, 4096], P(None, 'dp')
- next_inner: bfloat16 [2, 16, 3, 8192], P(None, 'dp', None, 'tp')
- next_write: bfloat16 [2, 16, 3, 2048], P(None, 'dp', None, 'tp')
- next_read: bfloat16 [2, 16, 3, 2048], P(None, 'dp', None, 'tp')
- next_recurrent: float32 [2, 16, 128, 64, 128], P(None, 'dp', 'tp')
Inputs may be any that keep to these rules, and one draw needn't show every extreme that they name: recurrent states of order a tenth, with scales that differ between heads.
All inputs are finite; a program needn't handle non-finite values.
Results may differ from a plain program's by a relative error of at most 0.025.
Values may be sent and summed in bfloat16 or wider, within the bound.
A program may use at most 64 MiB of HBM per device.

v0:
```python
import jax
import jax.numpy as jnp
from jax import lax
from jax.sharding import PartitionSpec as P

D = 4096
HEADS = 128
GROUPS = 16
eps = 1e-06


def convolve(state, fresh_row, kernel):
    window = jnp.concatenate([state, fresh_row[:, None, :]], axis=1)
    summed = jnp.sum(window.astype(jnp.float32) * kernel.astype(jnp.float32)[None], axis=1)
    return (jax.nn.silu(summed), window[:, 1:])


def mixer_block(normed, number, weights):
    (
        gate_weight,
        inner_weight,
        write_weight,
        read_weight,
        step_weight,
        conv_inner,
        conv_write,
        conv_read,
        step_bias,
        decay_log,
        skip_gain,
        group_gain,
        out_weight,
        state_inner,
        state_write,
        state_read,
        recurrent,
    ) = weights

    def partial_of(weight):
        return jnp.dot(normed, weight[number], preferred_element_type=jnp.float32).astype(
            jnp.bfloat16
        )

    summed = (
        lax.psum_scatter(partial_of(gate_weight), "dp", scatter_dimension=0, tiled=True).astype(
            jnp.float32
        ),
        lax.psum_scatter(partial_of(inner_weight), "dp", scatter_dimension=0, tiled=True).astype(
            jnp.float32
        ),
        lax.psum_scatter(partial_of(write_weight), "dp", scatter_dimension=0, tiled=True).astype(
            jnp.float32
        ),
        lax.psum_scatter(partial_of(read_weight), "dp", scatter_dimension=0, tiled=True).astype(
            jnp.float32
        ),
        lax.psum_scatter(partial_of(step_weight), "dp", scatter_dimension=0, tiled=True).astype(
            jnp.float32
        ),
    )
    gate_raw, inner_raw, write_raw, read_raw, step_raw = [
        member.astype(jnp.bfloat16) for member in summed
    ]
    inner_act, next_inner = convolve(state_inner[number], inner_raw, conv_inner[number])
    write_act, next_write = convolve(state_write[number], write_raw, conv_write[number])
    read_act, next_read = convolve(state_read[number], read_raw, conv_read[number])
    write_all, read_all = (
        lax.all_gather(write_act.astype(jnp.bfloat16), "tp", axis=1, tiled=True),
        lax.all_gather(read_act.astype(jnp.bfloat16), "tp", axis=1, tiled=True),
    )
    heads_here = step_bias.shape[1]
    head_dim = recurrent.shape[3]
    state_dim = recurrent.shape[4]
    rows_here = inner_act.shape[0]
    first_head = lax.axis_index("tp") * heads_here
    group_index = first_head // (HEADS // GROUPS)
    write_grid = write_all.reshape(rows_here, state_dim, GROUPS)
    read_grid = read_all.reshape(rows_here, state_dim, GROUPS)
    write_vec = lax.dynamic_slice_in_dim(write_grid, group_index, 1, 2)[:, :, 0].astype(jnp.float32)
    read_vec = lax.dynamic_slice_in_dim(read_grid, group_index, 1, 2)[:, :, 0].astype(jnp.float32)
    step_own = lax.dynamic_slice_in_dim(step_raw, first_head, heads_here, 1)
    step_size = jax.nn.softplus(step_own.astype(jnp.float32) + step_bias[number][None, :])
    retain = jnp.exp(-step_size * jnp.exp(decay_log[number])[None, :])
    inner_heads = inner_act.reshape(rows_here, heads_here, head_dim)
    updated = (
        retain[:, :, None, None] * recurrent[number]
        + (step_size[:, :, None] * inner_heads)[:, :, :, None] * write_vec[:, None, None, :]
    )
    readout = jnp.einsum("bhpn,bn->bhp", updated, read_vec, precision=lax.Precision.HIGHEST)
    readout = readout + skip_gain[number][None, :, None] * inner_heads
    gated_out = readout.reshape(rows_here, heads_here * head_dim) * jax.nn.silu(
        gate_raw.astype(jnp.float32)
    )
    selector = (jnp.arange(GROUPS) == group_index).astype(jnp.float32)
    totals = lax.psum(jnp.sum(gated_out * gated_out, axis=1)[:, None] * selector[None, :], "tp")
    group_sum = jnp.sum(totals * selector[None, :], axis=1, keepdims=True)
    group_factor = lax.rsqrt(group_sum / (HEADS // GROUPS * head_dim) + eps)
    group_normed = (gated_out * group_factor * group_gain[number][None, :]).astype(jnp.bfloat16)
    branch = jnp.dot(
        lax.all_gather(group_normed, "dp", axis=0, tiled=True),
        out_weight[number],
        preferred_element_type=jnp.float32,
    )
    return (branch, (next_inner, next_write, next_read, updated))


def total_over(branch):
    return lax.psum(branch, "tp")


def local(
    hidden,
    norm_gain,
    gate_weight,
    inner_weight,
    write_weight,
    read_weight,
    step_weight,
    conv_inner,
    conv_write,
    conv_read,
    step_bias,
    decay_log,
    skip_gain,
    group_gain,
    out_weight,
    state_inner,
    state_write,
    state_read,
    recurrent,
):
    weights = (
        gate_weight,
        inner_weight,
        write_weight,
        read_weight,
        step_weight,
        conv_inner,
        conv_write,
        conv_read,
        step_bias,
        decay_log,
        skip_gain,
        group_gain,
        out_weight,
        state_inner,
        state_write,
        state_read,
        recurrent,
    )
    wide_in = hidden.astype(jnp.float32)
    squares = lax.psum(jnp.sum(wide_in * wide_in, axis=1, keepdims=True), "dp")
    normed = (wide_in * lax.rsqrt(squares / D + eps) * norm_gain[0][None, :]).astype(jnp.bfloat16)
    branch, first_states = mixer_block(normed, 0, weights)
    middle = (wide_in + total_over(branch)).astype(jnp.bfloat16).astype(jnp.float32)
    squares = lax.psum(jnp.sum(middle * middle, axis=1, keepdims=True), "dp")
    normed = (middle * lax.rsqrt(squares / D + eps) * norm_gain[1][None, :]).astype(jnp.bfloat16)
    branch, second_states = mixer_block(normed, 1, weights)
    result = (middle + total_over(branch)).astype(jnp.bfloat16)
    stacked = [jnp.stack([earlier, later]) for earlier, later in zip(first_states, second_states)]
    return (result, stacked[0], stacked[1], stacked[2], stacked[3])


def solution(mesh):
    return jax.shard_map(
        local,
        mesh=mesh,
        in_specs=(
            P(None, "dp"),
            P(None, "dp"),
            P(None, "dp", "tp"),
            P(None, "dp", "tp"),
            P(None, "dp", "tp"),
            P(None, "dp", "tp"),
            P(None, "dp", None),
            P(None, None, "tp"),
            P(None, None, "tp"),
            P(None, None, "tp"),
            P(None, "tp"),
            P(None, "tp"),
            P(None, "tp"),
            P(None, "tp"),
            P(None, "tp", "dp"),
            P(None, "dp", None, "tp"),
            P(None, "dp", None, "tp"),
            P(None, "dp", None, "tp"),
            P(None, "dp", "tp", None, None),
        ),
        out_specs=(
            P(None, "dp"),
            P(None, "dp", None, "tp"),
            P(None, "dp", None, "tp"),
            P(None, "dp", None, "tp"),
            P(None, "dp", "tp", None, None),
        ),
        check_vma=False,
    )
```

profile of v0, /device:TPU:0, one launch (start us, length us, event | category | flops | bytes accessed | tf_op | source)
XLA Modules:
  0.0 509.0 jit_solution(9227752754220769065)
XLA Ops:
  7.2 1.0 fusion.58
  8.2 2.6 psum.42
  10.8 0.8 fusion.97
  11.8 2.8 fusion.28
  14.7 2.6 fusion.31
  19.3 1.3 convolution_convert_fusion.5
  20.6 3.5 all-reduce.7
  24.2 42.2 %all_gather.18 = bf16[8,2048]{1,0:T(8,128)(2,1)S(1)} all-gather(bf16[8,128]{1,0:T(8,128)(2,1)S(1)} %multiply_convert_fusion.5), channel_id=1, replica_groups=mesh['tp'=16,'dp'=2] {'tp'}, dimensions={1}, use_global_device_ids=true | all-gather | bytes 34816 | tf_op jit(solution)/shard_map/all_gather | solution.py:68
  66.4 35.6 %all_gather.19 = bf16[8,2048]{1,0:T(8,128)(2,1)S(1)} all-gather(bf16[8,128]{1,0:T(8,128)(2,1)S(1)} %multiply_convert_fusion.4), channel_id=1, replica_groups=mesh['tp'=16,'dp'=2] {'tp'}, dimensions={1}, use_global_device_ids=true | all-gather | bytes 34816 | tf_op jit(solution)/shard_map/all_gather | solution.py:69
  104.0 4.2 fusion.16
  108.4 0.8 multiply_reduce_fusion.5
  109.3 38.6 %psum.43 = f32[8,16]{1,0:T(8,128)S(1)} all-reduce(f32[8,16]{1,0:T(8,128)S(1)} %broadcast_multiply_fusion.3), channel_id=1, replica_groups=mesh['tp'=16,'dp'=2] {'tp'}, use_global_device_ids=true, to_apply=%region_11.12 | all-reduce | flops 128 | bytes 1024 | tf_op jit(solution)/shard_map/psum | solution.py:95
  148.8 1.8 all_gather.20
  150.6 2.6 fusion.9
  153.4 101.5 %all-reduce.11.cloned.1.call-done = f32[16,2048]{1,0:T(8,128)} async-done(((f32[16,2048]{1,0:T(8,128)}), f32[16,2048]{1,0:T(8,128)}) %all-reduce.11.cloned.1.call-update) | async-done | bytes 131088 | tf_op jit(solution)/shard_map/psum | solution.py:108
  254.8 1.0 fusion.62
  255.9 2.5 psum.45
  258.8 1.3 convolution_convert_fusion.2
  260.1 2.6 fusion.34
  262.8 2.6 fusion.37
  265.4 3.3 all-reduce.6
  270.1 38.9 %all_gather.21 = bf16[8,2048]{1,0:T(8,128)(2,1)S(1)} all-gather(bf16[8,128]{1,0:T(8,128)(2,1)S(1)} %multiply_convert_fusion.3), channel_id=1, replica_groups=mesh['tp'=16,'dp'=2] {'tp'}, dimensions={1}, use_global_device_ids=true | all-gather | bytes 34816 | tf_op jit(solution)/shard_map/all_gather | solution.py:68
  309.1 35.6 %all_gather.22 = bf16[8,2048]{1,0:T(8,128)(2,1)S(1)} all-gather(bf16[8,128]{1,0:T(8,128)(2,1)S(1)} %multiply_convert_fusion.2), channel_id=1, replica_groups=mesh['tp'=16,'dp'=2] {'tp'}, dimensions={1}, use_global_device_ids=true | all-gather | bytes 34816 | tf_op jit(solution)/shard_map/all_gather | solution.py:69
  346.6 4.2 multiply_add_fusion.1
  350.8 2.8 fusion.7
  353.8 0.8 multiply_reduce_fusion.2
  354.7 39.1 %psum.46 = f32[8,16]{1,0:T(8,128)S(1)} all-reduce(f32[8,16]{1,0:T(8,128)S(1)} %broadcast_multiply_fusion.2), channel_id=1, replica_groups=mesh['tp'=16,'dp'=2] {'tp'}, use_global_device_ids=true, to_apply=%region_25.26 | all-reduce | flops 128 | bytes 1024 | tf_op jit(solution)/shard_map/psum | solution.py:95
  394.7 1.8 all_gather.23
  396.5 2.6 fusion
  399.1 4.1 pad_maximum_fusion
  403.8 96.8 %all-reduce.13.cloned.1.call-done = f32[16,2048]{1,0:T(8,128)} async-done(((f32[16,2048]{1,0:T(8,128)}), f32[16,2048]{1,0:T(8,128)}) %all-reduce.13.cloned.1.call-update) | async-done | bytes 131088 | tf_op jit(solution)/shard_map/psum | solution.py:108
  500.6 1.6 fusion.65
  (117 shorter events, 10.1 us)
Async XLA Ops:
  7.2 7.5 %copy-start.1 = (bf16[16,2048]{1,0:T(8,128)(2,1)S(1)}, bf16[16,2048]{1,0:T(8,128)(2,1)}, u32[]{:S(2)}) copy-start(bf16[16,2048]{1,0:T(8,128)(2,1)} %param.19) | copy-start | bytes 196612
  7.2 96.0 %reduce-scatter.5.cloned.1.call-start = ((), (), s32[]{:S(2)}) async-start(), calls=%async_computation.4 | async-start | bytes 24576 | tf_op jit(solution)/shard_map/reduce_scatter | solution.py:48
  11.7 5.8 %copy-start.16 = (u32[32]{0:T(128)S(1)}, u32[32]{0:T(128)}, u32[]{:S(2)}) copy-start(u32[32]{0:T(128)} %constant.63) | copy-start | bytes 388
  11.7 7.0 %copy-start.11 = (f32[2,8]{1,0:T(2,128)S(1)}, f32[2,8]{1,0:T(2,128)}, u32[]{:S(2)}) copy-start(f32[2,8]{1,0:T(2,128)} %param.31) | copy-start | bytes 196
  11.7 7.0 %copy-start.9 = (bf16[2,4,128]{2,1,0:T(4,128)(2,1)S(1)}, bf16[2,4,128]{2,1,0:T(4,128)(2,1)}, u32[]{:S(2)}) copy-start(bf16[2,4,128]{2,1,0:T(4,128)(2,1)} %param.27) | copy-start | bytes 6148
  11.7 7.0 %copy-start.10 = (bf16[2,4,128]{2,1,0:T(4,128)(2,1)S(1)}, bf16[2,4,128]{2,1,0:T(4,128)(2,1)}, u32[]{:S(2)}) copy-start(bf16[2,4,128]{2,1,0:T(4,128)(2,1)} %param.28) | copy-start | bytes 6148
  11.7 7.0 %copy-start.8 = (f32[2,512]{1,0:T(2,128)S(1)}, f32[2,512]{1,0:T(2,128)}, u32[]{:S(2)}) copy-start(f32[2,512]{1,0:T(2,128)} %param.32) | copy-start | bytes 12292
  11.7 7.1 %copy-start.5 = (bf16[2,8,3,128]{3,1,2,0:T(8,128)(2,1)S(1)}, bf16[2,8,3,128]{3,1,2,0:T(8,128)(2,1)}, u32[]{:S(2)}) copy-start(bf16[2,8,3,128]{3,1,2,0:T(8,128)(2,1)} %param.35) | copy-start | bytes 36868
  11.7 7.1 %copy-start.6 = (bf16[2,8,3,128]{3,1,2,0:T(8,128)(2,1)S(1)}, bf16[2,8,3,128]{3,1,2,0:T(8,128)(2,1)}, u32[]{:S(2)}) copy-start(bf16[2,8,3,128]{3,1,2,0:T(8,128)(2,1)} %param.36) | copy-start | bytes 36868
  11.7 7.1 %copy-start.14 = (bf16[2,2048,128]{2,1,0:T(8,128)(2,1)S(1)}, bf16[2,2048,128]{2,1,0:T(8,128)(2,1)}, u32[]{:S(2)}) copy-start(bf16[2,2048,128]{2,1,0:T(8,128)(2,1)} %param.23) | copy-start | bytes 3145732
  11.8 7.3 %copy-start.15 = (bf16[2,2048,128]{2,1,0:T(8,128)(2,1)S(1)}, bf16[2,2048,128]{2,1,0:T(8,128)(2,1)}, u32[]{:S(2)}) copy-start(bf16[2,2048,128]{2,1,0:T(8,128)(2,1)} %param.24) | copy-start | bytes 3145732
  14.6 9.5 %copy-start.7 = (bf16[2,4,512]{2,1,0:T(4,128)(2,1)S(1)}, bf16[2,4,512]{2,1,0:T(4,128)(2,1)}, u32[]{:S(2)}) copy-start(bf16[2,4,512]{2,1,0:T(4,128)(2,1)} %param.26) | copy-start | bytes 24580
  14.6 87.4 %copy-start.2 = (bf16[2,8,3,512]{3,1,2,0:T(8,128)(2,1)S(1)}, bf16[2,8,3,512]{3,1,2,0:T(8,128)(2,1)}, u32[]{:S(2)}) copy-start(bf16[2,8,3,512]{3,1,2,0:T(8,128)(2,1)} %param.34) | copy-start | bytes 147460
  14.6 93.8 %reduce-scatter.7.cloned.1.call-start = ((), (), s32[]{:S(2)}) async-start(), calls=%async_computation.5 | async-start | bytes 24576 | tf_op jit(solution)/shard_map/reduce_scatter | solution.py:45
  17.3 85.7 %copy-start.12 = (f32[2,8]{1,0:T(2,128)S(1)}, f32[2,8]{1,0:T(2,128)}, u32[]{:S(2)}) copy-start(f32[2,8]{1,0:T(2,128)} %param.30) | copy-start | bytes 196
  17.3 85.7 %copy-start.13 = (f32[2,8]{1,0:T(2,128)S(1)}, f32[2,8]{1,0:T(2,128)}, u32[]{:S(2)}) copy-start(f32[2,8]{1,0:T(2,128)} %param.29) | copy-start | bytes 196
  17.3 237.5 %all-reduce.11.cloned.1.call-start = ((), (), s32[]{:S(2)}) async-start(), calls=%async_computation.6 | async-start | bytes 262144 | tf_op jit(solution)/shard_map/psum | solution.py:108
  104.0 49.3 %copy-start.3 = (bf16[8,512]{1,0:T(8,128)(2,1)S(1)}, bf16[8,512]{1,0:T(8,128)(2,1)}, u32[]{:S(2)}) copy-start(bf16[8,512]{1,0:T(8,128)(2,1)} %reduce-scatter.5.cloned.1.call-done) | copy-start | bytes 24580
  153.3 192.4 %reduce-scatter.9.cloned.1.call-start = ((), (), s32[]{:S(2)}) async-start(), calls=%async_computation.7 | async-start | bytes 24576 | tf_op jit(solution)/shard_map/reduce_scatter | solution.py:48
  268.8 85.0 %reduce-scatter.11.cloned.1.call-start = ((), (), s32[]{:S(2)}) async-start(), calls=%async_computation.8 | async-start | bytes 24576 | tf_op jit(solution)/shard_map/reduce_scatter | solution.py:45
  345.5 155.1 %all-reduce.13.cloned.1.call-start = ((), (), s32[]{:S(2)}) async-start(), calls=%async_computation.9 | async-start | bytes 262144 | tf_op jit(solution)/shard_map/psum | solution.py:108
  346.6 4.2 copy-start
  399.1 4.1 copy-start.4
Sparse Core Ops, SparseCore 0:
  14.7 10.0 reduce-scatter.4
  27.6 8.6 reduce-scatter.6
  153.4 101.3 all-reduce.10
  268.9 6.5 reduce-scatter.8
  345.7 5.2 reduce-scatter.10
  399.3 101.3 all-reduce.12
where the time goes:
time: 510 us; the launch traced here: 509 us
  blocking collectives  245 us (48%)
  waiting for transfers between devices  198 us (39%)
  matrix products  26.6 us (5%)
  other arithmetic  19.8 us (4%)
  between operations  15.3 us (3%)
    psum x2, waiting for transfers between devices, total_over(): return lax.psum(branch, 'tp')  198 us
    all_gather x2, blocking collectives, mixer_block(): lax.all_gather(write_act.astype(jnp.bfloat16), 'tp', axis=1, tiled=True)  81.1 us
    psum x2, blocking collectives, mixer_block(): lax.psum(jnp.sum(gated_out * gated_out, axis=1)[:, None] * selector[None,...  77.7 us
    all_gather x2, blocking collectives, mixer_block(): lax.all_gather(read_act.astype(jnp.bfloat16), 'tp', axis=1, tiled=True)  71.2 us
    dot_general x10, matrix products, partial_of(): jnp.dot(normed, weight[number], preferred_element_type=jnp.float32)  14.2 us
  transfers between devices with their start and end apart: 6, of which 2 were waited for; matrix products, arithmetic and copies ran while one was open for 5% of the time, Pallas kernels for 0%

commit v1 on v0

--- a/solution.py
+++ b/solution.py
@@ -64,9 +64,16 @@
     inner_act, next_inner = convolve(state_inner[number], inner_raw, conv_inner[number])
     write_act, next_write = convolve(state_write[number], write_raw, conv_write[number])
     read_act, next_read = convolve(state_read[number], read_raw, conv_read[number])
+
+    def _wrap_thing(vector, mesh_ax):
+        moved = tuple((vector for _ in range(lax.axis_size(mesh_ax))))
+        z2 = lax.all_to_all(jnp.stack(moved, 0), axis_name=mesh_ax, split_axis=0, concat_axis=0)
+        u1 = jnp.concatenate(z2, 1)
+        return u1
+
     write_all, read_all = (
         lax.all_gather(write_act.astype(jnp.bfloat16), "tp", axis=1, tiled=True),
-        lax.all_gather(read_act.astype(jnp.bfloat16), "tp", axis=1, tiled=True),
+        _wrap_thing(read_act.astype(jnp.bfloat16), "tp"),
     )
     heads_here = step_bias.shape[1]
     head_dim = recurrent.shape[3]

time: 510 us -> 456 us (0.89)
  blocking collectives: 245 us -> 171 us
  starting transfers between devices: 0.25 us -> 12.9 us
  waiting for transfers between devices: 198 us -> 206 us
    all_gather x2 -> x0, blocking collectives: 71.2 us -> none  [mixer_block(): lax.all_gather(read_act.astype(jnp.bfloat16), 'tp', axis=1, tiled=True)]
    all_to_all x0 -> x2, starting transfers between devices: none -> 12.7 us  [_wrap_thing(): lax.all_to_all(jnp.stack(moved, 0), axis_name=mesh_ax, split_axis=0, conc...]
    psum x2, waiting for transfers between devices: 198 us -> 206 us  [total_over(): return lax.psum(branch, 'tp')]
  transfers between devices with their start and end apart: 6 -> 8, of which waited for: 2 -> 2; matrix products, arithmetic and copies ran while one was open for 5% -> 6% of each run, Pallas kernels for 0% -> 0%
where the time goes in v1:
time: 456 us; the launch traced here: 455 us
  waiting for transfers between devices  206 us (45%)
  blocking collectives  171 us (38%)
  matrix products  27.8 us (6%)
  other arithmetic  17.7 us (4%)
  between operations  15.4 us (3%)
  starting transfers between devices  12.9 us (3%)
    psum x2, waiting for transfers between devices, total_over(): return lax.psum(branch, 'tp')  206 us
    all_gather x2, blocking collectives, mixer_block(): lax.all_gather(write_act.astype(jnp.bfloat16), 'tp', axis=1, tiled=True)  82.2 us
    psum x2, blocking collectives, mixer_block(): lax.psum(jnp.sum(gated_out * gated_out, axis=1)[:, None] * selector[None,...  73.1 us
    dot_general x10, matrix products, partial_of(): jnp.dot(normed, weight[number], preferred_element_type=jnp.float32)  14.1 us
    all_to_all x2, starting transfers between devices, _wrap_thing(): lax.all_to_all(jnp.stack(moved, 0), axis_name=mesh_ax, split_axis=0, conc...  12.7 us
  transfers between devices with their start and end apart: 8, of which 2 were waited for; matrix products, arithmetic and copies ran while one was open for 6% of the time, Pallas kernels for 0%

profile of v1, /device:TPU:0, one launch (start us, length us, event | category | flops | bytes accessed | tf_op | source)
XLA Modules:
  0.0 455.3 jit_solution(13492545874779061188)
XLA Ops:
  7.3 1.1 fusion.58
  8.4 2.6 psum.42
  11.0 0.8 fusion.97
  11.8 2.7 fusion.28
  15.2 1.3 convolution_convert_fusion.5
  17.7 3.5 all-reduce.7
  21.8 8.0 %all-to-all-start = ((bf16[16,8,128]{2,1,0:T(8,128)(2,1)}), bf16[16,8,128]{2,1,0:T(8,128)(2,1)S(1)}, u32[]{:S(2)}, u32[]{:S(2)}) async-start(bf16[16,8,128]{2,1,0:T(8,128)(2,1)} %stack.24), calls=%async_computation.1 | async-start | bytes 65536 | tf_op jit(solution)/shard_map/all_to_all | solution.py:70
  29.9 2.6 fusion.31
  32.8 41.1 %all_gather.12 = bf16[8,2048]{1,0:T(8,128)(2,1)S(1)} all-gather(bf16[8,128]{1,0:T(8,128)(2,1)S(1)} %multiply_convert_fusion.5), channel_id=1, replica_groups=mesh['tp'=16,'dp'=2] {'tp'}, dimensions={1}, use_global_device_ids=true | all-gather | bytes 34816 | tf_op jit(solution)/shard_map/all_gather | solution.py:75
  76.0 4.2 fusion.16
  80.4 0.8 multiply_reduce_fusion.5
  81.3 36.5 %psum.43 = f32[8,16]{1,0:T(8,128)S(1)} all-reduce(f32[8,16]{1,0:T(8,128)S(1)} %broadcast_multiply_fusion.3), channel_id=1, replica_groups=mesh['tp'=16,'dp'=2] {'tp'}, use_global_device_ids=true, to_apply=%region_11.12 | all-reduce | flops 128 | bytes 1024 | tf_op jit(solution)/shard_map/psum | solution.py:102
  118.7 1.8 all_gather.13
  120.5 2.6 fusion.9
  123.3 103.3 %all-reduce.11.cloned.1.call-done = f32[16,2048]{1,0:T(8,128)} async-done(((f32[16,2048]{1,0:T(8,128)}), f32[16,2048]{1,0:T(8,128)}) %all-reduce.11.cloned.1.call-update) | async-done | bytes 131088 | tf_op jit(solution)/shard_map/psum | solution.py:115
  226.6 1.0 fusion.62
  227.6 2.5 psum.45
  230.6 1.3 convolution_convert_fusion.2
  231.9 2.6 fusion.34
  234.5 2.6 fusion.37
  237.1 3.3 all-reduce.6
  241.2 4.7 %all-to-all-start.1 = ((bf16[16,8,128]{2,1,0:T(8,128)(2,1)}), bf16[16,8,128]{2,1,0:T(8,128)(2,1)S(1)}, u32[]{:S(2)}, u32[]{:S(2)}) async-start(bf16[16,8,128]{2,1,0:T(8,128)(2,1)} %stack.25), calls=%async_computation.4 | async-start | bytes 65536 | tf_op jit(solution)/shard_map/all_to_all | solution.py:70
  247.1 41.1 %all_gather.14 = bf16[8,2048]{1,0:T(8,128)(2,1)S(1)} all-gather(bf16[8,128]{1,0:T(8,128)(2,1)S(1)} %multiply_convert_fusion.3), channel_id=1, replica_groups=mesh['tp'=16,'dp'=2] {'tp'}, dimensions={1}, use_global_device_ids=true | all-gather | bytes 34816 | tf_op jit(solution)/shard_map/all_gather | solution.py:75
  289.7 3.7 multiply_add_fusion.1
  293.4 2.3 pad_maximum_fusion
  296.3 4.2 fusion.7
  300.6 0.8 multiply_reduce_fusion.2
  301.5 36.5 %psum.46 = f32[8,16]{1,0:T(8,128)S(1)} all-reduce(f32[8,16]{1,0:T(8,128)S(1)} %broadcast_multiply_fusion.2), channel_id=1, replica_groups=mesh['tp'=16,'dp'=2] {'tp'}, use_global_device_ids=true, to_apply=%region_25.26 | all-reduce | flops 128 | bytes 1024 | tf_op jit(solution)/shard_map/psum | solution.py:102
  339.0 1.8 all_gather.15
  340.8 2.6 fusion
  344.1 102.8 %all-reduce.13.cloned.1.call-done = f32[16,2048]{1,0:T(8,128)} async-done(((f32[16,2048]{1,0:T(8,128)}), f32[16,2048]{1,0:T(8,128)}) %all-reduce.13.cloned.1.call-update) | async-done | bytes 131088 | tf_op jit(solution)/shard_map/psum | solution.py:115
  446.9 1.6 fusion.65
  (121 shorter events, 11.3 us)
Async XLA Ops:
  7.2 7.4 %copy-start = (bf16[16,2048]{1,0:T(8,128)(2,1)S(1)}, bf16[16,2048]{1,0:T(8,128)(2,1)}, u32[]{:S(2)}) copy-start(bf16[16,2048]{1,0:T(8,128)(2,1)} %param.19) | copy-start | bytes 196612
  7.2 7.4 %copy-start.8 = (bf16[2,4,128]{2,1,0:T(4,128)(2,1)S(1)}, bf16[2,4,128]{2,1,0:T(4,128)(2,1)}, u32[]{:S(2)}) copy-start(bf16[2,4,128]{2,1,0:T(4,128)(2,1)} %param.28) | copy-start | bytes 6148
  7.2 7.4 %copy-start.4 = (bf16[2,8,3,128]{3,1,2,0:T(8,128)(2,1)S(1)}, bf16[2,8,3,128]{3,1,2,0:T(8,128)(2,1)}, u32[]{:S(2)}) copy-start(bf16[2,8,3,128]{3,1,2,0:T(8,128)(2,1)} %param.36) | copy-start | bytes 36868
  7.2 7.4 %copy-start.13 = (bf16[2,2048,128]{2,1,0:T(8,128)(2,1)S(1)}, bf16[2,2048,128]{2,1,0:T(8,128)(2,1)}, u32[]{:S(2)}) copy-start(bf16[2,2048,128]{2,1,0:T(8,128)(2,1)} %param.23) | copy-start | bytes 3145732
  7.2 7.7 %copy-start.14 = (bf16[2,2048,128]{2,1,0:T(8,128)(2,1)S(1)}, bf16[2,2048,128]{2,1,0:T(8,128)(2,1)}, u32[]{:S(2)}) copy-start(bf16[2,2048,128]{2,1,0:T(8,128)(2,1)} %param.24) | copy-start | bytes 3145732
  7.2 67.4 %reduce-scatter.5.cloned.1.call-start = ((), (), s32[]{:S(2)}) async-start(), calls=%async_computation.6 | async-start | bytes 24576 | tf_op jit(solution)/shard_map/reduce_scatter | solution.py:48
  11.8 4.6 %copy-start.15 = (u32[32]{0:T(128)S(1)}, u32[32]{0:T(128)}, u32[]{:S(2)}) copy-start(u32[32]{0:T(128)} %constant.63) | copy-start | bytes 388
  14.6 18.1 %copy-start.10 = (f32[2,8]{1,0:T(2,128)S(1)}, f32[2,8]{1,0:T(2,128)}, u32[]{:S(2)}) copy-start(f32[2,8]{1,0:T(2,128)} %param.31) | copy-start | bytes 196
  14.6 18.1 %copy-start.9 = (bf16[2,4,128]{2,1,0:T(4,128)(2,1)S(1)}, bf16[2,4,128]{2,1,0:T(4,128)(2,1)}, u32[]{:S(2)}) copy-start(bf16[2,4,128]{2,1,0:T(4,128)(2,1)} %param.27) | copy-start | bytes 6148
  14.6 18.1 %copy-start.7 = (f32[2,512]{1,0:T(2,128)S(1)}, f32[2,512]{1,0:T(2,128)}, u32[]{:S(2)}) copy-start(f32[2,512]{1,0:T(2,128)} %param.32) | copy-start | bytes 12292
  14.6 18.1 %copy-start.5 = (bf16[2,8,3,128]{3,1,2,0:T(8,128)(2,1)S(1)}, bf16[2,8,3,128]{3,1,2,0:T(8,128)(2,1)}, u32[]{:S(2)}) copy-start(bf16[2,8,3,128]{3,1,2,0:T(8,128)(2,1)} %param.35) | copy-start | bytes 36868
  14.6 18.1 %copy-start.6 = (bf16[2,4,512]{2,1,0:T(4,128)(2,1)S(1)}, bf16[2,4,512]{2,1,0:T(4,128)(2,1)}, u32[]{:S(2)}) copy-start(bf16[2,4,512]{2,1,0:T(4,128)(2,1)} %param.26) | copy-start | bytes 24580
  14.9 59.0 %copy-start.1 = (bf16[2,8,3,512]{3,1,2,0:T(8,128)(2,1)S(1)}, bf16[2,8,3,512]{3,1,2,0:T(8,128)(2,1)}, u32[]{:S(2)}) copy-start(bf16[2,8,3,512]{3,1,2,0:T(8,128)(2,1)} %param.34) | copy-start | bytes 147460
  14.9 59.3 %copy-start.11 = (f32[2,8]{1,0:T(2,128)S(1)}, f32[2,8]{1,0:T(2,128)}, u32[]{:S(2)}) copy-start(f32[2,8]{1,0:T(2,128)} %param.30) | copy-start | bytes 196
  14.9 59.3 %copy-start.12 = (f32[2,8]{1,0:T(2,128)S(1)}, f32[2,8]{1,0:T(2,128)}, u32[]{:S(2)}) copy-start(f32[2,8]{1,0:T(2,128)} %param.29) | copy-start | bytes 196
  21.8 53.6 %all-to-all-start = ((bf16[16,8,128]{2,1,0:T(8,128)(2,1)}), bf16[16,8,128]{2,1,0:T(8,128)(2,1)S(1)}, u32[]{:S(2)}, u32[]{:S(2)}) async-start(bf16[16,8,128]{2,1,0:T(8,128)(2,1)} %stack.24), calls=%async_computation.1 | async-start | bytes 65536 | tf_op jit(solution)/shard_map/all_to_all | solution.py:70
  29.9 50.5 %reduce-scatter.7.cloned.1.call-start = ((), (), s32[]{:S(2)}) async-start(), calls=%async_computation.7 | async-start | bytes 24576 | tf_op jit(solution)/shard_map/reduce_scatter | solution.py:45
  32.6 194.0 %all-reduce.11.cloned.1.call-start = ((), (), s32[]{:S(2)}) async-start(), calls=%async_computation.8 | async-start | bytes 262144 | tf_op jit(solution)/shard_map/psum | solution.py:115
  76.0 47.3 %copy-start.2 = (bf16[8,512]{1,0:T(8,128)(2,1)S(1)}, bf16[8,512]{1,0:T(8,128)(2,1)}, u32[]{:S(2)}) copy-start(bf16[8,512]{1,0:T(8,128)(2,1)} %reduce-scatter.5.cloned.1.call-done) | copy-start | bytes 24580
  123.2 165.7 %reduce-scatter.9.cloned.1.call-start = ((), (), s32[]{:S(2)}) async-start(), calls=%async_computation.9 | async-start | bytes 24576 | tf_op jit(solution)/shard_map/reduce_scatter | solution.py:48
  241.2 54.6 %all-to-all-start.1 = ((bf16[16,8,128]{2,1,0:T(8,128)(2,1)}), bf16[16,8,128]{2,1,0:T(8,128)(2,1)S(1)}, u32[]{:S(2)}, u32[]{:S(2)}) async-start(bf16[16,8,128]{2,1,0:T(8,128)(2,1)} %stack.25), calls=%async_computation.4 | async-start | bytes 65536 | tf_op jit(solution)/shard_map/all_to_all | solution.py:70
  245.8 54.8 %reduce-scatter.11.cloned.1.call-start = ((), (), s32[]{:S(2)}) async-start(), calls=%async_computation.10 | async-start | bytes 24576 | tf_op jit(solution)/shard_map/reduce_scatter | solution.py:45
  288.7 158.2 %all-reduce.13.cloned.1.call-start = ((), (), s32[]{:S(2)}) async-start(), calls=%async_computation.11 | async-start | bytes 262144 | tf_op jit(solution)/shard_map/psum | solution.py:115
  296.2 47.2 %copy-start.3 = (bf16[8,512]{1,0:T(8,128)(2,1)S(1)}, bf16[8,512]{1,0:T(8,128)(2,1)}, u32[]{:S(2)}) copy-start(bf16[8,512]{1,0:T(8,128)(2,1)} %reduce-scatter.9.cloned.1.call-done) | copy-start | bytes 24580
Sparse Core Ops, SparseCore 0:
  14.7 10.0 reduce-scatter.4
  33.4 8.7 reduce-scatter.6
  123.3 103.2 all-reduce.10
  240.7 6.5 reduce-scatter.8
  288.8 3.3 reduce-scatter.10
  343.6 103.2 all-reduce.12
